TPU v7x, 32 devices: a whole 2x2x4 slice. The times are simulated.
32 devices in a mesh: fs: 8 (over z, y), tp: 4 (over x, core).
Axes of the slice: x: 2, y: 2, z: 4, core: 2. Of those that a mesh axis runs over, the one named last changes fastest.
Arguments:
- tokens: bfloat16 [6144, 2048], P(('fs', 'tp')), may hold values from -60 to 60
- norm_gain: float32 [2048], P('fs'), may hold values from 0.1 to 1.9
- gate_weight: float32 [2048, 5632], P('fs', 'tp'), may hold values from -0.125 to 0.125
- up_weight: float32 [2048, 5632], P('fs', 'tp'), may hold values from -0.125 to 0.125
- down_weight: float32 [2048, 5632], P('fs', 'tp'), may hold values from -0.078125 to 0.078125
Outputs:
- mixed_rows: bfloat16 [6144, 2048], P(('fs', 'tp'))
- gate_out: bfloat16 [2048, 5632], P(None, 'tp')
- up_out: bfloat16 [2048, 5632], P(None, 'tp')
- down_out: bfloat16 [2048, 5632], P(None, 'tp')
All inputs are finite; a program needn't handle non-finite values.
Results may differ from a plain program's by a relative error of at most 0.014.
Values may be sent and summed in bfloat16 or wider, within the bound.
A program may use at most 128 MiB of HBM per device.

v0:
```python
import jax
import jax.numpy as jnp
from jax import lax
from jax.sharding import PartitionSpec as P


def normalize(source):
    widened = source.astype(jnp.float32)
    return (widened * lax.rsqrt(jnp.mean(widened * widened, axis=1, keepdims=True) + 1e-06)).astype(
        jnp.bfloat16
    )


def shards(tokens, norm_gain, gate_weight, up_weight, down_weight):
    row_gain = norm_gain[:, None]
    gate_local = (gate_weight * row_gain).astype(jnp.bfloat16)
    up_local = (up_weight * row_gain).astype(jnp.bfloat16)
    down_local = down_weight.astype(jnp.bfloat16)
    normed = normalize(tokens)
    gathered = lax.all_gather(normed, "tp", axis=0, tiled=True)
    down_whole = lax.all_gather(down_local, "fs", axis=0, tiled=True)
    gate_piece = lax.all_gather(gate_local, "fs", axis=0, tiled=True)
    up_piece = lax.all_gather(up_local, "fs", axis=0, tiled=True)
    gate_acc = jnp.dot(gathered, gate_piece, preferred_element_type=jnp.float32)
    up_acc = jnp.dot(gathered, up_piece, preferred_element_type=jnp.float32)
    hidden = (jax.nn.silu(gate_acc) * up_acc).astype(jnp.bfloat16)
    partial_value = lax.dot_general(
        hidden, down_whole, (((1,), (1,)), ((), ())), preferred_element_type=jnp.float32
    )
    mixed_rows = lax.psum_scatter(
        lax.optimization_barrier(partial_value.astype(jnp.bfloat16))
        .astype(jnp.float32)
        .astype(jnp.bfloat16),
        "tp",
        scatter_dimension=0,
        tiled=True,
    )
    return (mixed_rows, gate_piece, up_piece, down_whole)


def solution(mesh):
    in_specs = (P(("fs", "tp"), None), P("fs"), P("fs", "tp"), P("fs", "tp"), P("fs", "tp"))
    out_specs = (P(("fs", "tp"), None), P(None, "tp"), P(None, "tp"), P(None, "tp"))
    return jax.shard_map(shards, mesh=mesh, in_specs=in_specs, out_specs=out_specs, check_vma=False)
```

profile of v0, /device:TPU:0, one launch (start us, length us, event | category | flops | bytes accessed | tf_op | source)
XLA Modules:
  0.0 397.9 jit_solution(9030108663980922372)
XLA Ops:
  7.2 0.0 copy-start
  7.2 0.0 all-gather.5.cloned.1.call-start
  7.2 1.5 fusion
  8.7 2.2 fusion.1
  10.9 0.0 all-gather.5.cloned.1.call-update
  10.9 0.0 all-gather.7.cloned.1.call-start
  11.0 3.2 multiply_convert_fusion.1
  14.2 0.0 all-gather.7.cloned.1.call-update
  14.2 0.0 all-gather.11.cloned.1.call-start
  14.2 0.0 copy-done
  14.2 0.9 convert_element_type.28
  15.2 0.0 all-gather.11.cloned.1.call-update
  15.2 0.0 all-gather.9.cloned.1.call-start
  15.3 0.5 all-gather.9.cloned.1.call-update
  15.8 0.0 reduce-scatter.2.cloned.1.call-start
  15.8 26.5 %all-gather.5.cloned.1.call-done = bf16[768,2048]{1,0:T(8,128)(2,1)} async-done(((bf16[192,2048]{1,0:T(8,128)(2,1)}), bf16[768,2048]{1,0:T(8,128)(2,1)}) %all-gather.5.cloned.1.call-update) | async-done | bytes 3145744 | tf_op jit(solution)/shard_map/all_gather | solution.py:20
  42.3 0.0 copy-start.1
  42.3 95.1 %all-gather.7.cloned.1.call-done = bf16[2048,1408]{1,0:T(8,128)(2,1)} async-done(((bf16[256,1408]{1,0:T(8,128)(2,1)}), bf16[2048,1408]{1,0:T(8,128)(2,1)}) %all-gather.7.cloned.1.call-update) | async-done | bytes 5767184 | tf_op jit(solution)/shard_map/all_gather | solution.py:22
  137.4 9.7 %fusion.3 = f32[768,1408]{1,0:T(8,128)} fusion(bf16[768,2048]{1,0:T(8,128)(2,1)} %all-gather.5.cloned.1.call-done, bf16[2048,1408]{1,0:T(8,128)(2,1)} %all-gather.7.cloned.1.call-done), kind=kOutput, calls=%fused_computation.10 | convolution fusion | flops 4429185024 | bytes 13238272 | tf_op jit(solution)/shard_map/dot_general | solution.py:24
  147.1 83.6 %all-gather.11.cloned.1.call-done = bf16[2048,1408]{1,0:T(8,128)(2,1)} async-done(((bf16[256,1408]{1,0:T(8,128)(2,1)}), bf16[2048,1408]{1,0:T(8,128)(2,1)}) %all-gather.11.cloned.1.call-update) | async-done | bytes 5767184 | tf_op jit(solution)/shard_map/all_gather | solution.py:21
  230.7 93.1 %all-gather.9.cloned.1.call-done = bf16[2048,1408]{1,0:T(8,128)(2,1)} async-done(((bf16[256,1408]{1,0:T(8,128)(2,1)}), bf16[2048,1408]{1,0:T(8,128)(2,1)}) %all-gather.9.cloned.1.call-update) | async-done | bytes 5767184 | tf_op jit(solution)/shard_map/all_gather | solution.py:23
  323.8 0.0 copy-done.1
  323.8 17.3 %convolution_convert_fusion = bf16[768,2048]{1,0:T(8,128)(2,1)} fusion(bf16[2048,1408]{1,0:T(8,128)(2,1)} %all-gather.11.cloned.1.call-done, f32[768,1408]{1,0:T(8,128)} %fusion.3, bf16[768,2048]{1,0:T(8,128)(2,1)S(1)} %copy-done.1, bf16[2048,1408]{1,0:T(8,128)(2,1)} %all-gather.9.cloned.1.call-done), kind=kOutput, calls=%fused_computation.1 | convolution fusion | flops 8866430976 | bytes 22151168 | tf_op jit(solution)/shard_map/dot_general | solution.py:27
  341.2 0.0 reduce-scatter.2.cloned.1.call-update
  341.2 36.2 %reduce-scatter.2.cloned.1.call-done = bf16[192,2048]{1,0:T(8,128)(2,1)} async-done(((bf16[768,2048]{1,0:T(8,128)(2,1)}), bf16[192,2048]{1,0:T(8,128)(2,1)}) %reduce-scatter.2.cloned.1.call-update) | async-done | bytes 786448 | tf_op jit(solution)/shard_map/reduce_scatter | solution.py:30
  377.4 0.0 slice-start
  377.4 5.7 %copy.12 = bf16[2048,1408]{1,0:T(8,128)(2,1)} copy(bf16[2048,1408]{1,0:T(8,128)(2,1)} %all-gather.7.cloned.1.call-done) | data formatting | bytes 11534336
  383.2 0.0 slice-start.1
  383.2 5.7 %copy.13 = bf16[2048,1408]{1,0:T(8,128)(2,1)} copy(bf16[2048,1408]{1,0:T(8,128)(2,1)} %all-gather.9.cloned.1.call-done) | data formatting | bytes 11534336
  388.9 0.0 slice-done
  388.9 0.0 slice-done.1
  388.9 2.5 copy.14
  (2 shorter events, 0.0 us)
Async XLA Ops:
  7.2 7.1 %copy-start = (f32[256,1408]{1,0:T(8,128)S(1)}, f32[256,1408]{1,0:T(8,128)}, u32[]{:S(2)}) copy-start(f32[256,1408]{1,0:T(8,128)} %param.9) | copy-start | bytes 4325380
  7.2 35.2 %all-gather.5.cloned.1.call-start = ((), (), s32[]{:S(2)}) async-start(), calls=%async_computation.1 | async-start | bytes 3932160 | tf_op jit(solution)/shard_map/all_gather | solution.py:20
  10.9 126.5 %all-gather.7.cloned.1.call-start = ((), (), s32[]{:S(2)}) async-start(), calls=%async_computation.2 | async-start | bytes 6488064 | tf_op jit(solution)/shard_map/all_gather | solution.py:22
  14.2 216.5 %all-gather.11.cloned.1.call-start = ((), (), s32[]{:S(2)}) async-start(), calls=%async_computation.4 | async-start | bytes 6488064 | tf_op jit(solution)/shard_map/all_gather | solution.py:21
  15.2 308.6 %all-gather.9.cloned.1.call-start = ((), (), s32[]{:S(2)}) async-start(), calls=%async_computation.3 | async-start | bytes 6488064 | tf_op jit(solution)/shard_map/all_gather | solution.py:23
  15.8 361.6 %reduce-scatter.2.cloned.1.call-start = ((), (), s32[]{:S(2)}) async-start(), calls=%async_computation.5 | async-start | bytes 3932160 | tf_op jit(solution)/shard_map/reduce_scatter | solution.py:30
  42.3 281.5 %copy-start.1 = (bf16[768,2048]{1,0:T(8,128)(2,1)S(1)}, bf16[768,2048]{1,0:T(8,128)(2,1)}, u32[]{:S(2)}) copy-start(bf16[768,2048]{1,0:T(8,128)(2,1)} %all-gather.5.cloned.1.call-done) | copy-start | bytes 9437188
  377.4 11.5 %slice-start = ((s8[5767168]{0:T(1024)(128)(4,1)}), s8[4194304]{0:T(1024)(128)(4,1)S(1)}, s32[]{:S(2)}) async-start(s8[5767168]{0:T(1024)(128)(4,1)} %bitcast.5), calls=%async_computation.6 | async-start | bytes 8388608
  383.2 5.7 %slice-start.1 = ((s8[5767168]{0:T(1024)(128)(4,1)}), s8[1572864]{0:T(1024)(128)(4,1)S(1)}, s32[]{:S(2)}) async-start(s8[5767168]{0:T(1024)(128)(4,1)} %bitcast.5), calls=%async_computation.7 | async-start | bytes 3145728
Sparse Core Ops, SparseCore 0:
  11.1 31.2 all-gather.4
  45.1 92.2 all-gather.6
  140.2 90.4 all-gather.10
  233.3 90.4 all-gather.8
  341.3 36.0 reduce-scatter.1
where the time goes:
time: 398 us
  waiting for transfers between devices  335 us (84%)
  matrix products  27 us (7%)
  local copies, waits for them, and re-layouts  14 us (4%)
  between operations  13.8 us (3%)
  other arithmetic  7.8 us (2%)
    all_gather x1, waiting for transfers between devices, shards(): gate_piece = lax.all_gather(gate_local, 'fs', axis=0, tiled=True)  95.1 us
    all_gather x1, waiting for transfers between devices, shards(): up_piece = lax.all_gather(up_local, 'fs', axis=0, tiled=True)  93.1 us
    all_gather x1, waiting for transfers between devices, shards(): down_whole = lax.all_gather(down_local, 'fs', axis=0, tiled=True)  83.6 us
    reduce_scatter x1, waiting for transfers between devices, shards(): lax.psum_scatter(lax.optimization_barrier(partial_value.astype(jnp.bfloat...  36.2 us
    all_gather x1, waiting for transfers between devices, shards(): gathered = lax.all_gather(normed, 'tp', axis=0, tiled=True)  26.5 us
    dot_general x1, matrix products, shards(): lax.dot_general(hidden, down_whole, (((1,), (1,)), ((), ())), preferred_e...  17.3 us
    unnamed x11, local copies, waits for them, and re-layouts  14 us
    dot_general x1, matrix products, shards(): gate_acc = jnp.dot(gathered, gate_piece, preferred_element_type=jnp.float32)  9.67 us
  transfers between devices with their start and end apart: 5, of which 5 were waited for; matrix products, arithmetic and copies ran while one was open for 3% of the time, Pallas kernels for 0%

commit v1 on v0

--- a/solution.py
+++ b/solution.py
@@ -2,6 +2,24 @@
 import jax.numpy as jnp
 from jax import lax
 from jax.sharding import PartitionSpec as P
+
+
+def case_open(field):
+    n = lax.psum(1, "fs")
+    panels = [(m, (m + 1) % n) for m in range(n)]
+
+    def name_the_limits(clean):
+        if len(clean) == n:
+            return clean
+        side_arr = lax.ppermute(clean[0], "fs", panels)
+        f_next = name_the_limits([side_arr, *clean])
+        return f_next
+
+    all_values = name_the_limits([field])
+    n_now = jnp.concatenate(all_values, axis=0)
+    before = lax.axis_index("fs")
+    opened = jnp.roll(n_now, (before + 1) * field.shape[0], axis=0)
+    return opened
 
 
 def normalize(source):
@@ -20,7 +38,7 @@
     gathered = lax.all_gather(normed, "tp", axis=0, tiled=True)
     down_whole = lax.all_gather(down_local, "fs", axis=0, tiled=True)
     gate_piece = lax.all_gather(gate_local, "fs", axis=0, tiled=True)
-    up_piece = lax.all_gather(up_local, "fs", axis=0, tiled=True)
+    up_piece = case_open(up_local)
     gate_acc = jnp.dot(gathered, gate_piece, preferred_element_type=jnp.float32)
     up_acc = jnp.dot(gathered, up_piece, preferred_element_type=jnp.float32)
     hidden = (jax.nn.silu(gate_acc) * up_acc).astype(jnp.bfloat16)

time: 398 us -> 357 us (0.90)
  waiting for transfers between devices: 335 us -> 280 us
  local copies, waits for them, and re-layouts: 14 us -> 24.1 us
    ppermute x0 -> x7, waiting for transfers between devices: none -> 193 us  [name_the_limits(): side_arr = lax.ppermute(clean[0], 'fs', panels)]
    all_gather x1, waiting for transfers between devices: 95.1 us -> 0.01 us  [shards(): gate_piece = lax.all_gather(gate_local, 'fs', axis=0, tiled=True)]
    all_gather x1 -> x0, waiting for transfers between devices: 93.1 us -> none  [shards(): up_piece = lax.all_gather(up_local, 'fs', axis=0, tiled=True)]
    all_gather x1, waiting for transfers between devices: 83.6 us -> 50.6 us  [shards(): down_whole = lax.all_gather(down_local, 'fs', axis=0, tiled=True)]
    all_gather x1, waiting for transfers between devices: 26.5 us -> 0.01 us  [shards(): gathered = lax.all_gather(normed, 'tp', axis=0, tiled=True)]
    unnamed x11 -> x25, local copies, waits for them, and re-layouts: 14 us -> 21 us
  transfers between devices with their start and end apart: 5 -> 11, of which waited for: 5 -> 9; matrix products, arithmetic and copies ran while one was open for 3% -> 7% of each run, Pallas kernels for 0% -> 0%
where the time goes in v1:
time: 357 us
  waiting for transfers between devices  280 us (78%)
  matrix products  26.4 us (7%)
  local copies, waits for them, and re-layouts  24.1 us (7%)
  between operations  13.9 us (4%)
  other arithmetic  8.82 us (2%)
    ppermute x7, waiting for transfers between devices, name_the_limits(): side_arr = lax.ppermute(clean[0], 'fs', panels)  193 us
    all_gather x1, waiting for transfers between devices, shards(): down_whole = lax.all_gather(down_local, 'fs', axis=0, tiled=True)  50.6 us
    reduce_scatter x1, waiting for transfers between devices, shards(): lax.psum_scatter(lax.optimization_barrier(partial_value.astype(jnp.bfloat...  36.2 us
    unnamed x25, local copies, waits for them, and re-layouts  21 us
    dot_general x1, matrix products, shards(): lax.dot_general(hidden, down_whole, (((1,), (1,)), ((), ())), preferred_e...  16.7 us
    dot_general x1, matrix products, shards(): gate_acc = jnp.dot(gathered, gate_piece, preferred_element_type=jnp.float32)  9.67 us
  transfers between devices with their start and end apart: 11, of which 9 were waited for; matrix products, arithmetic and copies ran while one was open for 7% of the time, Pallas kernels for 0%

profile of v1, /device:TPU:0, one launch (start us, length us, event | category | flops | bytes accessed | tf_op | source)
XLA Modules:
  0.0 356.7 jit_solution(11975395129454846170)
XLA Ops:
  7.2 1.4 fusion
  8.6 2.2 fusion.1
  10.9 2.9 multiply_convert_fusion.1
  13.9 3.0 collective-permute-start
  16.9 19.2 %collective-permute-done = bf16[256,1408]{1,0:T(8,128)(2,1)S(1)} collective-permute-done((bf16[256,1408]{1,0:T(8,128)(2,1)S(1)}, bf16[256,1408]{1,0:T(8,128)(2,1)S(1)}, u32[]{:S(2)}, u32[]{:S(2)}) %collective-permute-start) | collective-permute-done | bytes 720928 | tf_op jit(solution)/shard_map/ppermute | solution.py:14
  36.1 2.3 convert_element_type.28
  38.5 17.7 %collective-permute-done.1 = bf16[256,1408]{1,0:T(8,128)(2,1)S(1)} collective-permute-done((bf16[256,1408]{1,0:T(8,128)(2,1)S(1)}, bf16[256,1408]{1,0:T(8,128)(2,1)S(1)}, u32[]{:S(2)}, u32[]{:S(2)}) %collective-permute-start.1) | collective-permute-done | bytes 720928 | tf_op jit(solution)/shard_map/ppermute | solution.py:14
  56.1 36.2 %collective-permute-done.2 = bf16[256,1408]{1,0:T(8,128)(2,1)S(1)} collective-permute-done((bf16[256,1408]{1,0:T(8,128)(2,1)S(1)}, bf16[256,1408]{1,0:T(8,128)(2,1)S(1)}, u32[]{:S(2)}, u32[]{:S(2)}) %collective-permute-start.2) | collective-permute-done | bytes 720928 | tf_op jit(solution)/shard_map/ppermute | solution.py:14
  92.4 26.3 %collective-permute-done.3 = bf16[256,1408]{1,0:T(8,128)(2,1)S(1)} collective-permute-done((bf16[256,1408]{1,0:T(8,128)(2,1)S(1)}, bf16[256,1408]{1,0:T(8,128)(2,1)S(1)}, u32[]{:S(2)}, u32[]{:S(2)}) %collective-permute-start.3) | collective-permute-done | bytes 720928 | tf_op jit(solution)/shard_map/ppermute | solution.py:14
  118.6 0.9 copy-done
  119.5 35.7 %collective-permute-done.4 = bf16[256,1408]{1,0:T(8,128)(2,1)S(1)} collective-permute-done((bf16[256,1408]{1,0:T(8,128)(2,1)S(1)}, bf16[256,1408]{1,0:T(8,128)(2,1)S(1)}, u32[]{:S(2)}, u32[]{:S(2)}) %collective-permute-start.4) | collective-permute-done | bytes 720928 | tf_op jit(solution)/shard_map/ppermute | solution.py:14
  155.2 0.9 copy-done.2
  156.1 34.4 %collective-permute-done.5 = bf16[256,1408]{1,0:T(8,128)(2,1)} collective-permute-done((bf16[256,1408]{1,0:T(8,128)(2,1)S(1)}, bf16[256,1408]{1,0:T(8,128)(2,1)}, u32[]{:S(2)}, u32[]{:S(2)}) %collective-permute-start.5) | collective-permute-done | bytes 720928 | tf_op jit(solution)/shard_map/ppermute | solution.py:14
  190.4 24.0 %collective-permute-done.6 = bf16[256,1408]{1,0:T(8,128)(2,1)} collective-permute-done((bf16[256,1408]{1,0:T(8,128)(2,1)}, bf16[256,1408]{1,0:T(8,128)(2,1)}, u32[]{:S(2)}, u32[]{:S(2)}) %collective-permute-start.6) | collective-permute-done | bytes 720928 | tf_op jit(solution)/shard_map/ppermute | solution.py:14
  214.5 1.2 constant_dynamic-update-slice_fusion.15
  215.6 1.2 constant_dynamic-update-slice_fusion.14
  216.9 1.3 constant_dynamic-update-slice_fusion.13
  218.1 1.3 constant_dynamic-update-slice_fusion.12
  219.4 0.1 constant_dynamic-update-slice_fusion.11
  219.5 0.1 constant_dynamic-update-slice_fusion.10
  219.6 0.1 constant_dynamic-update-slice_fusion.9
  219.7 0.1 constant_dynamic-update-slice_fusion.8
  219.8 1.2 constant_dynamic-update-slice_fusion.7
  221.0 1.2 constant_dynamic-update-slice_fusion.6
  222.2 0.1 constant_dynamic-update-slice_fusion.5
  222.8 3.0 constant_dynamic-slice_fusion
  225.8 9.7 %fusion.3 = f32[768,1408]{1,0:T(8,128)} fusion(bf16[768,2048]{1,0:T(8,128)(2,1)} %all-gather.4.cloned.1.call-done, bf16[2048,1408]{1,0:T(8,128)(2,1)} %all-gather.6.cloned.1.call-done), kind=kOutput, calls=%fused_computation.27 | convolution fusion | flops 4429185024 | bytes 13238272 | tf_op jit(solution)/shard_map/dot_general | solution.py:42
  235.4 50.6 %all-gather.8.cloned.1.call-done = bf16[2048,1408]{1,0:T(8,128)(2,1)} async-done(((bf16[256,1408]{1,0:T(8,128)(2,1)}), bf16[2048,1408]{1,0:T(8,128)(2,1)}) %all-gather.8.cloned.1.call-update) | async-done | bytes 5767184 | tf_op jit(solution)/shard_map/all_gather | solution.py:39
  286.1 16.7 %convolution_convert_fusion = bf16[768,2048]{1,0:T(8,128)(2,1)} fusion(bf16[2048,1408]{1,0:T(8,128)(2,1)} %all-gather.8.cloned.1.call-done, f32[768,1408]{1,0:T(8,128)} %fusion.3, bf16[768,2048]{1,0:T(8,128)(2,1)} %all-gather.4.cloned.1.call-done, bf16[2048,1408]{1,0:T(8,128)(2,1)} %constant_dynamic-slice_fusion), kind=kOutput, calls=%fused_computation.1 | convolution fusion | flops 8866430976 | bytes 22151168 | tf_op jit(solution)/shard_map/dot_general | solution.py:45
  302.8 36.2 %reduce-scatter.2.cloned.1.call-done = bf16[192,2048]{1,0:T(8,128)(2,1)} async-done(((bf16[768,2048]{1,0:T(8,128)(2,1)}), bf16[192,2048]{1,0:T(8,128)(2,1)}) %reduce-scatter.2.cloned.1.call-update) | async-done | bytes 786448 | tf_op jit(solution)/shard_map/reduce_scatter | solution.py:48
  339.0 5.6 %copy.26 = bf16[2048,1408]{1,0:T(8,128)(2,1)} copy(bf16[2048,1408]{1,0:T(8,128)(2,1)} %all-gather.6.cloned.1.call-done) | data formatting | bytes 11534336
  344.6 5.6 %copy.27 = bf16[2048,1408]{1,0:T(8,128)(2,1)} copy(bf16[2048,1408]{1,0:T(8,128)(2,1)} %all-gather.8.cloned.1.call-done) | data formatting | bytes 11534336
  (28 shorter events, 0.7 us)
Async XLA Ops:
  7.2 218.6 %all-gather.4.cloned.1.call-start = ((), (), s32[]{:S(2)}) async-start(), calls=%async_computation.1 | async-start | bytes 3932160 | tf_op jit(solution)/shard_map/all_gather | solution.py:38
  10.8 214.9 %all-gather.6.cloned.1.call-start = ((), (), s32[]{:S(2)}) async-start(), calls=%async_computation.2 | async-start | bytes 6488064 | tf_op jit(solution)/shard_map/all_gather | solution.py:40
  13.8 272.2 %all-gather.8.cloned.1.call-start = ((), (), s32[]{:S(2)}) async-start(), calls=%async_computation.3 | async-start | bytes 6488064 | tf_op jit(solution)/shard_map/all_gather | solution.py:39
  13.9 22.2 %collective-permute-start = (bf16[256,1408]{1,0:T(8,128)(2,1)S(1)}, bf16[256,1408]{1,0:T(8,128)(2,1)S(1)}, u32[]{:S(2)}, u32[]{:S(2)}) collective-permute-start(bf16[256,1408]{1,0:T(8,128)(2,1)S(1)} %get-tuple-element.4), channel_id=1, source_target_pairs={{0,4},{4,8},{8,12},{12,16},{16,20},{20,24},{24,28},{28,0},{1,5},{5... | collective-permute-start | bytes 2162696 | tf_op jit(solution)/shard_map/ppermute | solution.py:14
  36.1 20.0 %collective-permute-start.1 = (bf16[256,1408]{1,0:T(8,128)(2,1)S(1)}, bf16[256,1408]{1,0:T(8,128)(2,1)S(1)}, u32[]{:S(2)}, u32[]{:S(2)}) collective-permute-start(bf16[256,1408]{1,0:T(8,128)(2,1)S(1)} %collective-permute-done), channel_id=1, source_target_pairs={{0,4},{4,8},{8,12},{12,16},{16,20},{20,24},{24,28},{28,0},{1,5},{5... | collective-permute-start | bytes 2162696 | tf_op jit(solution)/shard_map/ppermute | solution.py:14
  38.4 300.6 %reduce-scatter.2.cloned.1.call-start = ((), (), s32[]{:S(2)}) async-start(), calls=%async_computation.4 | async-start | bytes 3932160 | tf_op jit(solution)/shard_map/reduce_scatter | solution.py:48
  56.1 36.2 %collective-permute-start.2 = (bf16[256,1408]{1,0:T(8,128)(2,1)S(1)}, bf16[256,1408]{1,0:T(8,128)(2,1)S(1)}, u32[]{:S(2)}, u32[]{:S(2)}) collective-permute-start(bf16[256,1408]{1,0:T(8,128)(2,1)S(1)} %collective-permute-done.1), channel_id=1, source_target_pairs={{0,4},{4,8},{8,12},{12,16},{16,20},{20,24},{24,28},{28,0},{1,5},{5... | collective-permute-start | bytes 2162696 | tf_op jit(solution)/shard_map/ppermute | solution.py:14
  92.4 26.3 %collective-permute-start.3 = (bf16[256,1408]{1,0:T(8,128)(2,1)S(1)}, bf16[256,1408]{1,0:T(8,128)(2,1)S(1)}, u32[]{:S(2)}, u32[]{:S(2)}) collective-permute-start(bf16[256,1408]{1,0:T(8,128)(2,1)S(1)} %collective-permute-done.2), channel_id=1, source_target_pairs={{0,4},{4,8},{8,12},{12,16},{16,20},{20,24},{24,28},{28,0},{1,5},{5... | collective-permute-start | bytes 2162696 | tf_op jit(solution)/shard_map/ppermute | solution.py:14
  118.6 0.9 copy-start
  119.5 35.7 %collective-permute-start.4 = (bf16[256,1408]{1,0:T(8,128)(2,1)S(1)}, bf16[256,1408]{1,0:T(8,128)(2,1)S(1)}, u32[]{:S(2)}, u32[]{:S(2)}) collective-permute-start(bf16[256,1408]{1,0:T(8,128)(2,1)S(1)} %collective-permute-done.3), channel_id=1, source_target_pairs={{0,4},{4,8},{8,12},{12,16},{16,20},{20,24},{24,28},{28,0},{1,5},{5... | collective-permute-start | bytes 2162696 | tf_op jit(solution)/shard_map/ppermute | solution.py:14
  155.2 0.9 copy-start.2
  156.1 34.4 %collective-permute-start.5 = (bf16[256,1408]{1,0:T(8,128)(2,1)S(1)}, bf16[256,1408]{1,0:T(8,128)(2,1)}, u32[]{:S(2)}, u32[]{:S(2)}) collective-permute-start(bf16[256,1408]{1,0:T(8,128)(2,1)S(1)} %collective-permute-done.4), channel_id=1, source_target_pairs={{0,4},{4,8},{8,12},{12,16},{16,20},{20,24},{24,28},{28,0},{1,5},{5... | collective-permute-start | bytes 2162696 | tf_op jit(solution)/shard_map/ppermute | solution.py:14
  190.4 24.0 %collective-permute-start.6 = (bf16[256,1408]{1,0:T(8,128)(2,1)}, bf16[256,1408]{1,0:T(8,128)(2,1)}, u32[]{:S(2)}, u32[]{:S(2)}) collective-permute-start(bf16[256,1408]{1,0:T(8,128)(2,1)} %collective-permute-done.5), channel_id=1, source_target_pairs={{0,4},{4,8},{8,12},{12,16},{16,20},{20,24},{24,28},{28,0},{1,5},{5... | collective-permute-start | bytes 2162696 | tf_op jit(solution)/shard_map/ppermute | solution.py:14
  216.8 5.4 %copy-start.3 = (bf16[256,1408]{1,0:T(8,128)(2,1)S(1)}, bf16[256,1408]{1,0:T(8,128)(2,1)}, u32[]{:S(2)}) copy-start(bf16[256,1408]{1,0:T(8,128)(2,1)} %copy-done.2) | copy-start | bytes 2162692
  218.1 4.2 %copy-start.1 = (bf16[256,1408]{1,0:T(8,128)(2,1)S(1)}, bf16[256,1408]{1,0:T(8,128)(2,1)}, u32[]{:S(2)}) copy-start(bf16[256,1408]{1,0:T(8,128)(2,1)} %copy-done) | copy-start | bytes 2162692
Sparse Core Ops, SparseCore 0:
  10.9 31.2 all-gather.3
  45.0 131.8 all-gather.5
  179.7 106.3 all-gather.7
  302.9 36.0 reduce-scatter.1
